TPU v7x, 32 devices: a whole 2x2x4 slice. The times are simulated.
32 devices in a mesh: ep: 4 (over y, x), tp: 8 (over z, core).
Axes of the slice: x: 2, y: 2, z: 4, core: 2. Of those that a mesh axis runs over, the one named last changes fastest.
Arguments:
- tokens: bfloat16 [128, 2048], P(('ep', 'tp')), may hold values from -6 to 6
- lengths: int32 [128], P(('ep', 'tp')), may hold values from 64 to 1024
- cache_latent: bfloat16 [128, 1024, 512], P(('ep', 'tp')), may hold values from -6 to 6
- cache_rope_key: bfloat16 [128, 1024, 32], P(('ep', 'tp')), may hold values from -1000 to 1000
- route_ids: int32 [128, 4], P('ep'), may hold values from 0 to 31, all different within a row; in each aligned block of 32 rows (0 to 31, 32 to 63, ...) at most 8 rows name the same one
- route_weights: float32 [128, 4], P('ep'), may hold values from 0.2 to 2
- attn_gain: float32 [2048], replicated, may hold values from 0.1 to 1.9
- w_query_nope: bfloat16 [2048, 16, 64], P(None, 'tp'), may hold values from -0.125 to 0.125
- w_query_rope: bfloat16 [2048, 16, 32], P(None, 'tp'), may hold values from -0.125 to 0.125
- w_latent_down: bfloat16 [2048, 512], P(None, 'tp'), may hold values from -0.125 to 0.125
- w_key_rope: bfloat16 [2048, 32], replicated, may hold values from -0.125 to 0.125
- latent_gain: float32 [512], replicated, may hold values from 0.1 to 1.9
- w_key_up: bfloat16 [512, 16, 64], P(None, 'tp'), may hold values from -0.75 to 0.75
- w_value_up: bfloat16 [512, 16, 64], P(None, 'tp'), may hold values from -0.25 to 0.25
- w_attn_out: bfloat16 [16, 64, 2048], P('tp'), may hold values from -0.1875 to 0.1875
- ffn_gain: float32 [2048], replicated, may hold values from 0.1 to 1.9
- expert_gate: bfloat16 [32, 2048, 512], P(('ep', 'tp')), may hold values from -0.125 to 0.125
- expert_up: bfloat16 [32, 2048, 512], P(('ep', 'tp')), may hold values from -0.125 to 0.125
- expert_down: bfloat16 [32, 512, 2048], P(('ep', 'tp')), may hold values from -0.25 to 0.25
- shared_gate: bfloat16 [2048, 512], P(None, 'tp'), may hold values from -0.125 to 0.125
- shared_up: bfloat16 [2048, 512], P(None, 'tp'), may hold values from -0.125 to 0.125
- shared_down: bfloat16 [512, 2048], P('tp'), may hold values from -0.25 to 0.25
- dense_gate: bfloat16 [2048, 1024], P(None, 'tp'), may hold values from -0.125 to 0.125
- dense_up: bfloat16 [2048, 1024], P(None, 'tp'), may hold values from -0.125 to 0.125
- dense_down: bfloat16 [1024, 2048], P('tp'), may hold values from -0.1875 to 0.1875
- branch_gate: bfloat16 [2048], replicated, may hold values from -0.125 to 0.125
Outputs:
- mixed: bfloat16 [128, 2048], P(('ep', 'tp'))
- new_latent: bfloat16 [128, 512], P(('ep', 'tp'))
- new_rope_key: bfloat16 [128, 32], P(('ep', 'tp'))
Inputs may be any that keep to these rules, and one draw needn't show every extreme that they name: `route_ids`: in each aligned block of 32 rows, no expert is named by more than 8 of the block's rows, a bound that some block reaches. Each row names 4 different experts.
All inputs are finite; a program needn't handle non-finite values.
Results may differ from a plain program's by a relative error of at most 0.025.
Values may be sent and summed in bfloat16 or wider, within the bound.
A program may use at most 64 MiB of HBM per device.

v0:
```python
import jax
import jax.numpy as jnp
from jax import lax
from jax.sharding import PartitionSpec as P

epsilon = 1e-06
rope_base = 10000.0


def norm_rows(values, scales):
    values = values.astype(jnp.float32)
    factor = lax.rsqrt(jnp.mean(values * values, axis=-1, keepdims=True) + epsilon)
    return values * factor * scales


def rotate(values, positions):
    half_dim = values.shape[-1] // 2
    frequencies = rope_base ** (-jnp.arange(half_dim).astype(jnp.float32) / half_dim)
    angles = positions.astype(jnp.float32)[:, None] * frequencies[None, :]
    bcast_shape = (angles.shape[0],) + (1,) * (values.ndim - 2) + (half_dim,)
    cosine = jnp.cos(angles).reshape(bcast_shape)
    sine_val = jnp.sin(angles).reshape(bcast_shape)
    first_half = values[..., :half_dim].astype(jnp.float32)
    second_half = values[..., half_dim:].astype(jnp.float32)
    return jnp.concatenate(
        [
            first_half * cosine - second_half * sine_val,
            first_half * sine_val + second_half * cosine,
        ],
        axis=-1,
    )


def swiglu(inputs, gate_w, up_w):
    gate_val = jnp.dot(inputs, gate_w, preferred_element_type=jnp.float32)
    up_val = jnp.dot(inputs, up_w, preferred_element_type=jnp.float32)
    return (jax.nn.silu(gate_val) * up_val).astype(jnp.bfloat16)


def local(
    tokens,
    lengths,
    cache_latent,
    cache_rope_key,
    route_ids,
    route_weights,
    attn_gain,
    w_query_nope,
    w_query_rope,
    w_latent_down,
    w_key_rope,
    latent_gain,
    w_key_up,
    w_value_up,
    w_attn_out,
    ffn_gain,
    expert_gate,
    expert_up,
    expert_down,
    shared_gate,
    shared_up,
    shared_down,
    dense_gate,
    dense_up,
    dense_down,
    branch_gate,
):
    own_rows, model_width = tokens.shape
    tp_count = lax.axis_size("tp")
    ep_count = lax.axis_size("ep")
    tp_index = lax.axis_index("tp")
    local_heads = w_query_nope.shape[1]
    head_scale = (w_query_nope.shape[2] + w_query_rope.shape[2]) ** (-0.5)
    normed = norm_rows(tokens, attn_gain).astype(jnp.bfloat16)
    group_in = lax.all_gather(normed, "tp", axis=0, tiled=True)
    group_rows = group_in.shape[0]
    query_nope = jnp.dot(
        group_in, w_query_nope.reshape(model_width, -1), preferred_element_type=jnp.float32
    )
    query_nope = query_nope.astype(jnp.bfloat16).reshape(group_rows, local_heads, -1)
    query_latent = jnp.einsum(
        "ghn,rhn->ghr", query_nope, w_key_up, preferred_element_type=jnp.float32
    ).astype(jnp.bfloat16)
    query_rope = jnp.dot(
        group_in, w_query_rope.reshape(model_width, -1), preferred_element_type=jnp.float32
    )
    query_rope = query_rope.astype(jnp.bfloat16).reshape(group_rows, local_heads, -1)
    latent_part = jnp.dot(group_in, w_latent_down, preferred_element_type=jnp.float32).astype(
        jnp.bfloat16
    )
    own_latent_q, own_rope_q, latent_raw = (
        lax.all_to_all(query_latent, "tp", split_axis=0, concat_axis=1, tiled=True),
        lax.all_to_all(query_rope, "tp", split_axis=0, concat_axis=1, tiled=True),
        lax.all_to_all(latent_part, "tp", split_axis=0, concat_axis=1, tiled=True),
    )
    new_latent = norm_rows(latent_raw, latent_gain).astype(jnp.bfloat16)
    key_rope = jnp.dot(normed, w_key_rope, preferred_element_type=jnp.float32)
    new_rope = rotate(key_rope, lengths).astype(jnp.bfloat16)
    query_rot = rotate(own_rope_q, lengths).astype(jnp.bfloat16)
    scores = jnp.einsum(
        "bhr,blr->bhl", own_latent_q, cache_latent, preferred_element_type=jnp.float32
    )
    scores = scores + jnp.einsum(
        "bhe,ble->bhl", query_rot, cache_rope_key, preferred_element_type=jnp.float32
    )
    scores = scores * head_scale
    in_range = (
        jnp.arange(cache_latent.shape[1], dtype=jnp.int32)[None, None, :] < lengths[:, None, None]
    )
    scores = jnp.where(in_range, scores, -jnp.inf)
    own_score = jnp.einsum(
        "bhr,br->bh", own_latent_q, new_latent, preferred_element_type=jnp.float32
    )
    own_score = (
        own_score
        + jnp.einsum("bhe,be->bh", query_rot, new_rope, preferred_element_type=jnp.float32)
    ) * head_scale
    peak_score = jnp.maximum(jnp.max(scores, axis=-1), own_score)
    past_exp = jnp.exp(scores - peak_score[..., None])
    own_exp = jnp.exp(own_score - peak_score)
    total_exp = jnp.sum(past_exp, axis=-1) + own_exp
    past_weight = (past_exp / total_exp[..., None]).astype(jnp.bfloat16)
    own_weight = (own_exp / total_exp).astype(jnp.bfloat16)
    out_latent = jnp.einsum(
        "bhl,blr->bhr", past_weight, cache_latent, preferred_element_type=jnp.float32
    )
    out_latent = (
        out_latent
        + own_weight.astype(jnp.float32)[..., None] * new_latent.astype(jnp.float32)[:, None, :]
    )
    out_latent = out_latent.astype(jnp.bfloat16)
    head_latent = lax.all_to_all(out_latent, "tp", split_axis=1, concat_axis=0, tiled=True)
    head_values = jnp.einsum(
        "ghr,rhv->ghv", head_latent, w_value_up, preferred_element_type=jnp.float32
    ).astype(jnp.bfloat16)
    attn_part = jnp.dot(
        head_values.reshape(group_rows, -1),
        w_attn_out.reshape(-1, model_width),
        preferred_element_type=jnp.float32,
    )
    own_start = tp_index * own_rows
    placed = lax.dynamic_update_slice_in_dim(
        jnp.zeros((group_rows, model_width), jnp.float32), tokens.astype(jnp.float32), own_start, 0
    )
    group_after = lax.psum((attn_part + placed).astype(jnp.bfloat16), "tp").astype(jnp.float32)
    ffn_in = norm_rows(group_after, ffn_gain).astype(jnp.bfloat16)
    after_attn = lax.dynamic_slice_in_dim(group_after, own_start, own_rows, 0)
    shared_term = jnp.dot(
        swiglu(ffn_in, shared_gate, shared_up), shared_down, preferred_element_type=jnp.float32
    )
    branch_mix = jax.nn.sigmoid(jnp.dot(ffn_in, branch_gate, preferred_element_type=jnp.float32))
    dense_term = branch_mix[:, None] * jnp.dot(
        swiglu(ffn_in, dense_gate, dense_up), dense_down, preferred_element_type=jnp.float32
    )
    top_count = route_ids.shape[1]
    expert_local = expert_gate.shape[0]
    capacity = max(
        2, (2 * own_rows * top_count + expert_local * ep_count - 1) // (expert_local * ep_count)
    )
    target_count = ep_count * expert_local
    slot_count = target_count * capacity
    column = route_ids // expert_local % tp_count
    target = route_ids // (expert_local * tp_count) * expert_local + route_ids % expert_local
    flat_target = jnp.where(column == tp_index, target, -1).reshape(-1)
    target_hits = (
        flat_target[:, None] == jnp.arange(target_count, dtype=jnp.int32)[None, :]
    ).astype(jnp.int32)
    earlier = jnp.cumsum(target_hits, axis=0) - target_hits
    rank_in = jnp.sum(earlier * target_hits, axis=1)
    slot_index = jnp.where(flat_target >= 0, flat_target * capacity + rank_in, -1).reshape(
        group_rows, top_count
    )
    slot_match = slot_index[:, :, None] == jnp.arange(slot_count, dtype=jnp.int32)[None, None, :]
    dispatch = jnp.any(slot_match, axis=1).astype(jnp.bfloat16)
    combine = jnp.sum(jnp.where(slot_match, route_weights[:, :, None], 0.0), axis=1)
    outgoing = jnp.einsum("gs,gd->sd", dispatch, ffn_in, preferred_element_type=jnp.float32).astype(
        jnp.bfloat16
    )
    outgoing = outgoing.reshape(ep_count, expert_local, capacity, model_width)
    arrived = lax.all_to_all(outgoing, "ep", split_axis=0, concat_axis=0, tiled=True)
    gate_val = jnp.einsum(
        "sxcd,xdf->sxcf", arrived, expert_gate, preferred_element_type=jnp.float32
    )
    up_val = jnp.einsum("sxcd,xdf->sxcf", arrived, expert_up, preferred_element_type=jnp.float32)
    act_val = (jax.nn.silu(gate_val) * up_val).astype(jnp.bfloat16)
    result = jnp.einsum(
        "sxcf,xfd->sxcd", act_val, expert_down, preferred_element_type=jnp.float32
    ).astype(jnp.bfloat16)
    returned = lax.all_to_all(result, "ep", split_axis=0, concat_axis=0, tiled=True)
    routed = jnp.dot(
        combine,
        returned.reshape(slot_count, model_width).astype(jnp.float32),
        precision=lax.Precision.HIGHEST,
    )
    ffn_total = routed + shared_term + dense_term
    mixed = (
        after_attn
        + lax.psum_scatter(
            ffn_total.astype(jnp.bfloat16), "tp", scatter_dimension=0, tiled=True
        ).astype(jnp.float32)
    ).astype(jnp.bfloat16)
    return (mixed, new_latent, new_rope)


def solution(mesh):
    in_specs = (
        P(("ep", "tp"), None),
        P(("ep", "tp")),
        P(("ep", "tp"), None, None),
        P(("ep", "tp"), None, None),
        P("ep", None),
        P("ep", None),
        P(),
        P(None, "tp", None),
        P(None, "tp", None),
        P(None, "tp"),
        P(),
        P(),
        P(None, "tp", None),
        P(None, "tp", None),
        P("tp", None, None),
        P(),
        P(("ep", "tp"), None, None),
        P(("ep", "tp"), None, None),
        P(("ep", "tp"), None, None),
        P(None, "tp"),
        P(None, "tp"),
        P("tp", None),
        P(None, "tp"),
        P(None, "tp"),
        P("tp", None),
        P(),
    )
    out_specs = (P(("ep", "tp"), None), P(("ep", "tp"), None), P(("ep", "tp"), None))
    return jax.shard_map(local, mesh=mesh, in_specs=in_specs, out_specs=out_specs, check_vma=False)
```

profile of v0, /device:TPU:0, one launch (start us, length us, event | category | flops | bytes accessed | tf_op | source)
XLA Modules:
  0.0 222.2 jit_solution(12282794214563576408)
XLA Ops:
  7.2 1.0 fusion.58
  8.2 0.8 fusion.95
  9.1 15.7 %all-gather = bf16[8,4,2048]{2,1,0:T(4,128)(2,1)S(1)} all-gather(bf16[1,4,2048]{2,1,0:T(4,128)(2,1)S(1)} %fusion.95), channel_id=1, replica_groups=mesh['ep'=4,'tp'=8] {'tp'}, dimensions={0}, use_global_device_ids=true | all-gather | bytes 147456 | tf_op jit(solution)/shard_map/all_gather | solution.py:75
  24.8 1.1 convolution_convert_fusion.5
  26.7 4.6 %all-to-all-start.2 = ((bf16[8,2,128]{2,1,0:T(2,128)(2,1)}), bf16[8,2,128]{2,1,0:T(2,128)(2,1)S(1)}, u32[]{:S(2)}, u32[]{:S(2)}) async-start(bf16[8,2,128]{2,1,0:T(2,128)(2,1)} %reshape.224), calls=%async_computation.2 | async-start | bytes 8192 | tf_op jit(solution)/shard_map/all_to_all | solution.py:94
  32.7 1.1 fusion.93
  35.3 1.1 convolution_convert_fusion.6
  36.4 1.3 convolution_convert_fusion.4
  41.6 5.1 %all-to-all-start.1 = ((bf16[8,2,128]{2,1,0:T(2,128)(2,1)}), bf16[8,2,128]{2,1,0:T(2,128)(2,1)S(1)}, u32[]{:S(2)}, u32[]{:S(2)}) async-start(bf16[8,2,128]{2,1,0:T(2,128)(2,1)} %reshape.222), calls=%async_computation.1 | async-start | bytes 8192 | tf_op jit(solution)/shard_map/all_to_all | solution.py:93
  47.0 5.2 %all-to-all-done.1 = bf16[8,2,128]{2,1,0:T(2,128)(2,1)S(1)} async-done(((bf16[8,2,128]{2,1,0:T(2,128)(2,1)}), bf16[8,2,128]{2,1,0:T(2,128)(2,1)S(1)}, u32[]{:S(2)}, u32[]{:S(2)}) %all-to-all-start.1) | async-done | bytes 4128 | tf_op jit(solution)/shard_map/all_to_all | solution.py:93
  52.2 3.3 %all-to-all-start = ((bf16[32,2,512]{2,1,0:T(2,128)(2,1)}), bf16[32,2,512]{2,1,0:T(2,128)(2,1)S(1)}, u32[]{:S(2)}, u32[]{:S(2)}) async-start(bf16[32,2,512]{2,1,0:T(2,128)(2,1)} %copy.64), calls=%async_computation | async-start | bytes 131072 | tf_op jit(solution)/shard_map/all_to_all | solution.py:92
  56.0 5.4 %all-to-all-done = bf16[32,2,512]{2,1,0:T(2,128)(2,1)S(1)} async-done(((bf16[32,2,512]{2,1,0:T(2,128)(2,1)}), bf16[32,2,512]{2,1,0:T(2,128)(2,1)S(1)}, u32[]{:S(2)}, u32[]{:S(2)}) %all-to-all-start) | async-done | bytes 65568 | tf_op jit(solution)/shard_map/all_to_all | solution.py:92
  61.7 3.5 %fusion.100 = f32[4,16,1024]{2,1,0:T(8,128)S(1)} fusion(bf16[4,16,512]{2,1,0:T(8,128)(2,1)S(1)} %all_to_all.58, bf16[4,1024,512]{2,1,0:T(8,128)(2,1)} %param.28), kind=kOutput, calls=%fused_computation.141 | convolution fusion | flops 67108864 | bytes 4521984 | tf_op jit(solution)/shard_map/bhr,blr->bhl/dot_general | solution.py:100
  67.2 3.3 %all-to-all-start.3 = ((bf16[4,16,512]{2,0,1:T(4,128)(2,1)}), bf16[4,16,512]{2,0,1:T(4,128)(2,1)S(1)}, u32[]{:S(2)}, u32[]{:S(2)}) async-start(bf16[4,16,512]{2,0,1:T(4,128)(2,1)} %copy.68), calls=%async_computation.3 | async-start | bytes 131072 | tf_op jit(solution)/shard_map/all_to_all | solution.py:132
  71.3 5.1 %all-to-all-done.3 = bf16[4,16,512]{2,0,1:T(4,128)(2,1)S(1)} async-done(((bf16[4,16,512]{2,0,1:T(4,128)(2,1)}), bf16[4,16,512]{2,0,1:T(4,128)(2,1)S(1)}, u32[]{:S(2)}, u32[]{:S(2)}) %all-to-all-start.3) | async-done | bytes 65568 | tf_op jit(solution)/shard_map/all_to_all | solution.py:132
  76.5 1.3 convolution_bitcast_fusion
  78.6 53.5 %all-reduce.4.cloned.1.call-done = bf16[32,2048]{1,0:T(8,128)(2,1)} async-done(((bf16[32,2048]{1,0:T(8,128)(2,1)}), bf16[32,2048]{1,0:T(8,128)(2,1)}) %all-reduce.4.cloned.1.call-update) | async-done | bytes 131088 | tf_op jit(solution)/shard_map/psum | solution.py:145
  132.1 1.0 multiply_reduce_fusion
  133.2 1.8 fusion.2
  135.0 3.6 %all-to-all-start.4 = ((bf16[4,1,8,2048]{3,2,1,0:T(8,128)(2,1)}), bf16[4,1,8,2048]{3,2,1,0:T(8,128)(2,1)S(1)}, u32[]{:S(2)}, u32[]{:S(2)}) async-start(bf16[4,1,8,2048]{3,2,1,0:T(8,128)(2,1)} %fusion.2), calls=%async_computation.4 | async-start | bytes 262144 | tf_op jit(solution)/shard_map/all_to_all | solution.py:180
  138.6 1.8 fusion.96
  140.4 1.9 fusion.97
  142.3 1.4 all-to-all-done.4
  143.7 2.0 fusion.13
  145.7 3.2 %fusion.3 = bf16[4,1,8,2048]{3,2,1,0:T(8,128)(2,1)} fusion(bf16[1,512,2048]{2,1,0:T(8,128)(2,1)S(1)} %copy-done, bf16[1,2048,512]{2,1,0:T(8,128)(2,1)} %param.43, bf16[4,1,8,2048]{3,2,1,0:T(8,128)(2,1)S(1)} %all-to-all-done.4, f32[4,1,8,512]{3,2,0,1:T(8,128)S(1)} %fusion.13), kind=kOutput, calls=%fused_computation.8 | convolution fusion | flops 134381568 | bytes 4521984 | tf_op jit(solution)/shard_map/sxcf,xfd->sxcd/dot_general | solution.py:186
  148.9 3.5 %all-to-all-start.5 = ((bf16[4,1,8,2048]{3,2,1,0:T(8,128)(2,1)}), bf16[4,1,8,2048]{3,2,1,0:T(8,128)(2,1)S(1)}, u32[]{:S(2)}, u32[]{:S(2)}) async-start(bf16[4,1,8,2048]{3,2,1,0:T(8,128)(2,1)} %fusion.3), calls=%async_computation.5 | async-start | bytes 262144 | tf_op jit(solution)/shard_map/all_to_all | solution.py:189
  153.2 4.2 %all-to-all-done.5 = bf16[4,1,8,2048]{3,2,1,0:T(8,128)(2,1)S(1)} async-done(((bf16[4,1,8,2048]{3,2,1,0:T(8,128)(2,1)}), bf16[4,1,8,2048]{3,2,1,0:T(8,128)(2,1)S(1)}, u32[]{:S(2)}, u32[]{:S(2)}) %all-to-all-start.5) | async-done | bytes 131104 | tf_op jit(solution)/shard_map/all_to_all | solution.py:189
  157.6 1.4 convolution_add_fusion
  159.1 2.2 fusion.1
  161.3 1.3 pad_maximum_fusion.3
  162.6 51.4 %all-reduce.6.cloned.1.call-done = bf16[32,2048]{1,0:T(8,128)(2,1)} async-done(((bf16[32,2048]{1,0:T(8,128)(2,1)}), bf16[32,2048]{1,0:T(8,128)(2,1)}) %all-reduce.6.cloned.1.call-update) | async-done | bytes 131088
  214.0 1.4 add_convert_fusion
  (96 shorter events, 12.4 us)
Async XLA Ops:
  7.2 138.5 %copy-start = (bf16[1,512,2048]{2,1,0:T(8,128)(2,1)S(1)}, bf16[1,512,2048]{2,1,0:T(8,128)(2,1)}, u32[]{:S(2)}) copy-start(bf16[1,512,2048]{2,1,0:T(8,128)(2,1)} %param.44) | copy-start | bytes 6291460
  7.2 33.2 %copy-start.18 = (u32[32]{0:T(128)S(1)}, u32[32]{0:T(128)}, u32[]{:S(2)}) copy-start(u32[32]{0:T(128)} %constant.109) | copy-start | bytes 388
  7.2 30.7 %copy-start.10 = (bf16[512,2,64]{0,2,1:T(8,128)(2,1)S(1)}, bf16[512,2,64]{0,2,1:T(8,128)(2,1)}, u32[]{:S(2)}) copy-start(bf16[512,2,64]{0,2,1:T(8,128)(2,1)} %param.38) | copy-start | bytes 393220
  7.2 31.0 %copy-start.14 = (bf16[2048]{0:T(1024)(128)(2,1)S(1)}, bf16[2048]{0:T(1024)(128)(2,1)}, u32[]{:S(2)}) copy-start(bf16[2048]{0:T(1024)(128)(2,1)} %param.51) | copy-start | bytes 12292
  7.2 48.5 %copy-start.16 = (f32[512]{0:T(512)S(1)}, f32[512]{0:T(512)}, u32[]{:S(2)}) copy-start(f32[512]{0:T(512)} %param.37) | copy-start | bytes 6148
  26.7 14.9 %all-to-all-start.2 = ((bf16[8,2,128]{2,1,0:T(2,128)(2,1)}), bf16[8,2,128]{2,1,0:T(2,128)(2,1)S(1)}, u32[]{:S(2)}, u32[]{:S(2)}) async-start(bf16[8,2,128]{2,1,0:T(2,128)(2,1)} %reshape.224), calls=%async_computation.2 | async-start | bytes 8192 | tf_op jit(solution)/shard_map/all_to_all | solution.py:94
  38.1 23.3 %copy-start.12 = (bf16[4,16]{1,0:T(4,128)(2,1)}, bf16[4,16]{1,0:T(4,128)(2,1)S(1)}, u32[]{:S(2)}) copy-start(bf16[4,16]{1,0:T(4,128)(2,1)S(1)} %get-tuple-element.10) | copy-start | bytes 388
  41.6 10.6 %all-to-all-start.1 = ((bf16[8,2,128]{2,1,0:T(2,128)(2,1)}), bf16[8,2,128]{2,1,0:T(2,128)(2,1)S(1)}, u32[]{:S(2)}, u32[]{:S(2)}) async-start(bf16[8,2,128]{2,1,0:T(2,128)(2,1)} %reshape.222), calls=%async_computation.1 | async-start | bytes 8192 | tf_op jit(solution)/shard_map/all_to_all | solution.py:93
  52.2 9.2 %all-to-all-start = ((bf16[32,2,512]{2,1,0:T(2,128)(2,1)}), bf16[32,2,512]{2,1,0:T(2,128)(2,1)S(1)}, u32[]{:S(2)}, u32[]{:S(2)}) async-start(bf16[32,2,512]{2,1,0:T(2,128)(2,1)} %copy.64), calls=%async_computation | async-start | bytes 131072 | tf_op jit(solution)/shard_map/all_to_all | solution.py:92
  55.8 9.4 %copy-start.15 = (bf16[4,512]{1,0:T(4,128)(2,1)}, bf16[4,512]{1,0:T(4,128)(2,1)S(1)}, u32[]{:S(2)}) copy-start(bf16[4,512]{1,0:T(4,128)(2,1)S(1)} %get-tuple-element.4) | copy-start | bytes 12292
  61.6 3.5 %copy-start.6 = (bf16[4,1024,32]{1,2,0:T(8,128)(2,1)S(1)}, bf16[4,1024,32]{1,2,0:T(8,128)(2,1)}, u32[]{:S(2)}) copy-start(bf16[4,1024,32]{1,2,0:T(8,128)(2,1)} %param.29) | copy-start | bytes 786436
  61.6 4.1 %copy-start.1 = (bf16[4,1024,512]{2,1,0:T(8,128)(2,1)S(1)}, bf16[4,1024,512]{2,1,0:T(8,128)(2,1)}, u32[]{:S(2)}) copy-start(bf16[4,1024,512]{2,1,0:T(8,128)(2,1)} %param.28) | copy-start | bytes 12582916
  65.8 4.8 %copy-start.17 = (f32[32,4]{0,1:T(4,128)S(1)}, f32[32,4]{0,1:T(4,128)}, u32[]{:S(2)}) copy-start(f32[32,4]{0,1:T(4,128)} %param.31) | copy-start | bytes 1540
  65.8 10.7 %copy-start.4 = (bf16[2,64,2048]{2,1,0:T(8,128)(2,1)S(1)}, bf16[2,64,2048]{2,1,0:T(8,128)(2,1)}, u32[]{:S(2)}) copy-start(bf16[2,64,2048]{2,1,0:T(8,128)(2,1)} %param.40) | copy-start | bytes 1572868
  65.8 12.0 %copy-start.9 = (bf16[4,2048]{1,0:T(4,128)(2,1)S(1)}, bf16[4,2048]{1,0:T(4,128)(2,1)}, u32[]{:S(2)}) copy-start(bf16[4,2048]{1,0:T(4,128)(2,1)} %param.26) | copy-start | bytes 49156
  66.5 66.7 %copy-start.8 = (f32[2048]{0:T(1024)S(1)}, f32[2048]{0:T(1024)}, u32[]{:S(2)}) copy-start(f32[2048]{0:T(1024)} %param.41) | copy-start | bytes 24580
  66.5 72.1 %copy-start.3 = (bf16[2048,128]{1,0:T(8,128)(2,1)S(1)}, bf16[2048,128]{1,0:T(8,128)(2,1)}, u32[]{:S(2)}) copy-start(bf16[2048,128]{1,0:T(8,128)(2,1)} %param.48) | copy-start | bytes 1572868
  67.2 9.2 %all-to-all-start.3 = ((bf16[4,16,512]{2,0,1:T(4,128)(2,1)}), bf16[4,16,512]{2,0,1:T(4,128)(2,1)S(1)}, u32[]{:S(2)}, u32[]{:S(2)}) async-start(bf16[4,16,512]{2,0,1:T(4,128)(2,1)} %copy.68), calls=%async_computation.3 | async-start | bytes 131072 | tf_op jit(solution)/shard_map/all_to_all | solution.py:132
  70.5 61.6 %all-reduce.4.cloned.1.call-start = ((), (), s32[]{:S(2)}) async-start(), calls=%async_computation.6 | async-start | bytes 262144 | tf_op jit(solution)/shard_map/psum | solution.py:145
  135.0 8.7 %all-to-all-start.4 = ((bf16[4,1,8,2048]{3,2,1,0:T(8,128)(2,1)}), bf16[4,1,8,2048]{3,2,1,0:T(8,128)(2,1)S(1)}, u32[]{:S(2)}, u32[]{:S(2)}) async-start(bf16[4,1,8,2048]{3,2,1,0:T(8,128)(2,1)} %fusion.2), calls=%async_computation.4 | async-start | bytes 262144 | tf_op jit(solution)/shard_map/all_to_all | solution.py:180
  145.7 6.7 %copy-start.2 = (bf16[32,2048]{1,0:T(8,128)(2,1)S(1)}, bf16[32,2048]{1,0:T(8,128)(2,1)}, u32[]{:S(2)}) copy-start(bf16[32,2048]{1,0:T(8,128)(2,1)} %all-reduce.4.cloned.1.call-done) | copy-start | bytes 393220
  145.7 6.7 %copy-start.13 = (bf16[2048,1]{0,1:T(2,128)(2,1)S(1)}, bf16[2048,1]{0,1:T(2,128)(2,1)}, u32[]{:S(2)}) copy-start(bf16[2048,1]{0,1:T(2,128)(2,1)} %reshape.219) | copy-start | bytes 12292
  145.7 11.7 %copy-start.11 = (f32[32,32]{1,0:T(8,128)S(1)}, f32[32,32]{1,0:T(8,128)}, u32[]{:S(2)}) copy-start(f32[32,32]{1,0:T(8,128)} %select_reduce_fusion) | copy-start | bytes 12292
  145.7 11.9 %copy-start.7 = (bf16[64,2048]{1,0:T(8,128)(2,1)S(1)}, bf16[64,2048]{1,0:T(8,128)(2,1)}, u32[]{:S(2)}) copy-start(bf16[64,2048]{1,0:T(8,128)(2,1)} %param.47) | copy-start | bytes 786436
  148.9 10.2 %copy-start.5 = (bf16[128,2048]{1,0:T(8,128)(2,1)S(1)}, bf16[128,2048]{1,0:T(8,128)(2,1)}, u32[]{:S(2)}) copy-start(bf16[128,2048]{1,0:T(8,128)(2,1)} %param.50) | copy-start | bytes 1572868
  148.9 8.4 %all-to-all-start.5 = ((bf16[4,1,8,2048]{3,2,1,0:T(8,128)(2,1)}), bf16[4,1,8,2048]{3,2,1,0:T(8,128)(2,1)S(1)}, u32[]{:S(2)}, u32[]{:S(2)}) async-start(bf16[4,1,8,2048]{3,2,1,0:T(8,128)(2,1)} %fusion.3), calls=%async_computation.5 | async-start | bytes 262144 | tf_op jit(solution)/shard_map/all_to_all | solution.py:189
  152.4 61.6 %all-reduce.6.cloned.1.call-start = ((), (), s32[]{:S(2)}) async-start(), calls=%async_computation.7 | async-start | bytes 262144
Sparse Core Ops, SparseCore 0:
  78.6 53.4 all-reduce.3
  161.4 52.5 all-reduce.5
where the time goes:
time: 223 us; the launch traced here: 222 us
  waiting for transfers between devices  126 us (57%)
  matrix products  26.3 us (12%)
  starting transfers between devices  23.6 us (11%)
  blocking collectives  15.7 us (7%)
  between operations  15.1 us (7%)
  other arithmetic  9.66 us (4%)
  local copies, waits for them, and re-layouts  5.69 us (3%)
    psum x1, waiting for transfers between devices, local(): lax.psum((attn_part + placed).astype(jnp.bfloat16), 'tp')  53.5 us
    unnamed x3, waiting for transfers between devices  51.4 us
    all_gather x1, blocking collectives, local(): group_in = lax.all_gather(normed, 'tp', axis=0, tiled=True)  15.7 us
    all_to_all x1, waiting for transfers between devices, local(): lax.all_to_all(query_latent, 'tp', split_axis=0, concat_axis=1, tiled=True)  5.38 us
    all_to_all x1, waiting for transfers between devices, local(): lax.all_to_all(query_rope, 'tp', split_axis=0, concat_axis=1, tiled=True)  5.2 us
    all_to_all x1, starting transfers between devices, local(): lax.all_to_all(query_rope, 'tp', split_axis=0, concat_axis=1, tiled=True)  5.11 us
    all_to_all x1, waiting for transfers between devices, local(): lax.all_to_all(out_latent, 'tp', split_axis=1, concat_axis=0, tiled=True)  5.08 us
    all_to_all x1, starting transfers between devices, local(): lax.all_to_all(latent_part, 'tp', split_axis=0, concat_axis=1, tiled=True)  4.6 us
  transfers between devices with their start and end apart: 8, of which 7 were waited for; matrix products, arithmetic and copies ran while one was open for 8% of the time, Pallas kernels for 0%

commit v1 on v0

v1 whole, which is shorter than its diff:
```python
import functools

import jax
import jax.numpy as jnp
from jax import lax
from jax.experimental import pallas as pl
from jax.experimental.pallas import tpu as pltpu
from jax.sharding import PartitionSpec as P

epsilon = 1e-06
rope_base = 10000.0
lanes = 128
F32 = jnp.float32
BF16 = jnp.bfloat16
MESH = pl.DeviceIdType.MESH


def nn(a, b):
    return lax.dot_general(a, b, (((1,), (0,)), ((), ())), preferred_element_type=F32)


def nt(a, b):
    return lax.dot_general(a, b, (((1,), (1,)), ((), ())), preferred_element_type=F32)


def tn(a, b):
    return lax.dot_general(a, b, (((0,), (0,)), ((), ())), preferred_element_type=F32)


def join(pieces):
    return pieces[0] if len(pieces) == 1 else jnp.concatenate(pieces, axis=0)


def rows_of(ref, count):
    return join([ref[i].astype(F32) for i in range(count)])


def factor_of(values):
    return lax.rsqrt(jnp.mean(values * values, axis=-1, keepdims=True) + epsilon)


def silu(v):
    return v / (1.0 + jnp.exp(-v))


def lane_block(values, column, width):
    base, offset = column // lanes * lanes, column % lanes
    block = values[:, base : base + lanes]
    if offset:
        block = pltpu.roll(block, lanes - offset, 1)
    lane = lax.broadcasted_iota(jnp.int32, block.shape, 1)
    return jnp.where(lane < width, block, 0.0)


def turn(values, cosine, sine, half):
    lane = lax.broadcasted_iota(jnp.int32, values.shape, 1)
    swapped = jnp.where(
        lane < half, -pltpu.roll(values, lanes - half, 1), pltpu.roll(values, half, 1)
    )
    return values * cosine + swapped * sine


def layer(
    sizes,
    consts, tab, tokens, ids, wts,
    wqn, wqr, wld, wkr, cl, cr, wku, wvu, wo, sg, su, dg, du, sd, dd, eg, eu, ed,
    mixed, newlat, newrope,
    v_in, v_kr, v_cl, v_cr, v_ku, v_vu, v_wo, v_sg, v_su, v_dg, v_du, v_sd, v_dd, v_eg, v_eu, v_ed,
    agx, sendq, recvq, sendo, recvo, senda, recva, agf, sende, recve, sendr, recvr, sendf, recvf,
    kr_pad, w_sem, tp_send, tp_recv, ep_send, ep_recv,
):
    T, EP, own, H, nope, rope, latent, cap, scale = sizes
    group = T * own
    R = H * own
    me_t = lax.axis_index("tp")
    me_e = lax.axis_index("ep")
    lat_w = wld.shape[0]

    barrier = pltpu.get_barrier_semaphore()
    for k in range(1, T):
        pl.semaphore_signal(
            barrier, inc=1, device_id=(me_e, lax.rem(me_t + k, T)), device_id_type=MESH
        )
    for k in range(1, EP):
        pl.semaphore_signal(
            barrier, inc=1, device_id=(lax.rem(me_e + k, EP), me_t), device_id_type=MESH
        )

    n_q, n_r = H * nope, H * rope
    pairs = [
        (wqn, v_in.at[pl.ds(0, n_q)]),
        (wqr, v_in.at[pl.ds(n_q, n_r)]),
        (wld, v_in.at[pl.ds(n_q + n_r, lat_w)]),
        (wkr, v_kr),
        (wku, v_ku),
    ]
    first_cl = len(pairs)
    pairs += [(cl.at[b], v_cl.at[b]) for b in range(own)]
    first_rest = len(pairs)
    pairs += [(cr, v_cr), (wvu, v_vu), (wo, v_wo)]
    first_ffn = len(pairs)
    pairs += [
        (sg, v_sg), (su, v_su), (dg, v_dg), (du, v_du), (sd, v_sd), (dd, v_dd),
        (eg, v_eg), (eu, v_eu), (ed, v_ed),
    ]
    loads = [
        pltpu.make_async_copy(src, dst, w_sem.at[i]) for i, (src, dst) in enumerate(pairs)
    ]
    for load in loads:
        load.start()

    sends = []

    def tp_exchange(phase, source, target):
        out = []
        for k in range(1, T):
            peer = lax.rem(me_t + k, T)
            out.append(
                pltpu.make_async_remote_copy(
                    src_ref=source(peer),
                    dst_ref=target.at[me_t],
                    send_sem=tp_send.at[phase, k],
                    recv_sem=tp_recv.at[phase, k],
                    device_id=(me_e, peer),
                    device_id_type=MESH,
                )
            )
        for c in out:
            c.start()
        sends.extend(out)
        return out

    def ep_exchange(phase, source, target):
        out = []
        for k in range(1, EP):
            peer = lax.rem(me_e + k, EP)
            out.append(
                pltpu.make_async_remote_copy(
                    src_ref=source.at[peer],
                    dst_ref=target.at[me_e],
                    send_sem=ep_send.at[phase, k],
                    recv_sem=ep_recv.at[phase, k],
                    device_id=(peer, me_t),
                    device_id_type=MESH,
                )
            )
        for c in out:
            c.start()
        sends.extend(out)
        return out

    def arrive(copies):
        for c in copies:
            c.wait_recv()

    x = tokens[...].astype(F32)
    normed = (x * factor_of(x) * consts[0:1, :]).astype(BF16)
    agx[me_t] = normed
    pl.semaphore_wait(barrier, T - 1 + EP - 1)
    step = tp_exchange(0, lambda peer: agx.at[me_t], agx)

    slots = EP * cap
    slot = lax.broadcasted_iota(jnp.int32, (slots, group), 0)
    block = jnp.zeros((slots, group), jnp.int32)
    for j in range(1, EP):
        block = block + jnp.where(slot >= j * cap, 1, 0)
    expert = block * T + me_t
    place = (slot - block * cap).astype(F32)
    hit = jnp.zeros((slots, group), F32)
    weight = jnp.zeros((slots, group), F32)
    for k in range(ids.shape[0]):
        same = ids[k : k + 1, :] == expert
        hit = hit + jnp.where(same, 1.0, 0.0)
        weight = weight + jnp.where(same, wts[k : k + 1, :], 0.0)
    upper = jnp.where(
        lax.broadcasted_iota(jnp.int32, (group, group), 0)
        < lax.broadcasted_iota(jnp.int32, (group, group), 1),
        1.0,
        0.0,
    ).astype(BF16)
    rank = nn(hit.astype(BF16), upper)
    dispatch = jnp.where(rank == place, hit, 0.0)
    weight = weight * dispatch
    weight_hi = weight.astype(BF16)
    weight_lo = (weight - weight_hi.astype(F32)).astype(BF16)
    dispatch = dispatch.astype(BF16)

    for i in range(first_cl):
        loads[i].wait()
    cosine, sine = tab[0], tab[1]
    kr_pad[...] = jnp.zeros_like(kr_pad)
    kr_pad[:, 0:rope] = nt(normed, v_kr[...])
    new_rope = turn(kr_pad[...], cosine[0:own], sine[0:own], rope // 2).astype(BF16)
    newrope[...] = new_rope[:, 0:rope]

    arrive(step)
    rows = rows_of(agx, T).astype(BF16)
    proj = nt(rows, v_in[...])
    q_lat = [
        nn(lane_block(proj, h * nope, nope)[:, 0:nope].astype(BF16), v_ku[h]) for h in range(H)
    ]
    q_rope = [lane_block(proj, n_q + h * rope, rope) for h in range(H)]
    lat_part = lane_block(proj, n_q + n_r, lat_w)
    for u in range(T):
        cut = slice(own * u, own * (u + 1))
        sendq[u, :, 0:latent] = join([q[cut] for q in q_lat]).astype(BF16)
        sendq[u, :, latent : latent + lanes] = join([q[cut] for q in q_rope]).astype(BF16)
        sendq[u, :, latent + lanes : latent + 2 * lanes] = join([lat_part[cut]] * H).astype(BF16)
    step = tp_exchange(1, lambda peer: sendq.at[peer], recvq)
    recvq[me_t] = sendq[me_t]
    for i in range(first_cl, first_ffn):
        loads[i].wait()
    arrive(step)

    queries = rows_of(recvq, T)
    q_all = queries[:, 0:latent].astype(BF16)
    q_rot = turn(queries[:, latent : latent + lanes], cosine, sine, rope // 2).astype(BF16)
    per = lanes // lat_w
    blocks = []
    for j in range(T // per):
        total = None
        for i in range(per):
            piece = queries[R * (j * per + i) : R * (j * per + i) + own, latent + lanes :]
            if i:
                piece = pltpu.roll(piece, i * lat_w, 1)
            total = piece if total is None else total + piece
        blocks.append(total)
    raw = blocks[0] if len(blocks) == 1 else jnp.concatenate(blocks, axis=1)
    new_latent = (raw * factor_of(raw) * consts[3:4, 0:latent]).astype(BF16)
    newlat[...] = new_latent
    lat_rows = join([new_latent.astype(F32)] * (T * H))
    rope_rows = join([new_rope.astype(F32)] * (T * H))
    own_score = (
        jnp.sum(q_all.astype(F32) * lat_rows, axis=-1, keepdims=True)
        + jnp.sum(q_rot.astype(F32) * rope_rows, axis=-1, keepdims=True)
    ) * scale
    length = tab[2][:, 0:1]
    which = tab[3][:, 0:1]
    scores = None
    for b in range(own):
        part = nt(q_all, v_cl[b]) + nn(q_rot[:, 0:rope], v_cr[b])
        scores = part if scores is None else jnp.where(which == float(b), part, scores)
    position = lax.broadcasted_iota(jnp.int32, scores.shape, 1).astype(F32)
    scores = jnp.where(position < length, scores * scale, -jnp.inf)
    peak = jnp.maximum(jnp.max(scores, axis=-1, keepdims=True), own_score)
    past = jnp.exp(scores - peak)
    own_exp = jnp.exp(own_score - peak)
    total = jnp.sum(past, axis=-1, keepdims=True) + own_exp
    past = (past / total).astype(BF16)
    own_weight = (own_exp / total).astype(BF16).astype(F32)
    mixed_lat = None
    for b in range(own):
        part = nn(past, v_cl[b])
        mixed_lat = part if mixed_lat is None else jnp.where(which == float(b), part, mixed_lat)
    mixed_lat = mixed_lat + own_weight * lat_rows
    for u in range(T):
        sendo[u] = mixed_lat[R * u : R * (u + 1)].astype(BF16)
    step = tp_exchange(2, lambda peer: sendo.at[peer], recvo)
    recvo[me_t] = sendo[me_t]
    arrive(step)

    back = rows_of(recvo, T).astype(BF16)
    part = None
    for h in range(H):
        values = nt(back, v_vu[h])
        values = join(
            [values[R * u + own * h : R * u + own * (h + 1)] for u in range(T)]
        ).astype(BF16)
        term = nn(values, v_wo[h])
        part = term if part is None else part + term
    for u in range(T):
        senda[u] = part[own * u : own * (u + 1)].astype(BF16)
    step = tp_exchange(3, lambda peer: senda.at[peer], recva)
    recva[me_t] = senda[me_t]
    arrive(step)
    after = tokens[...].astype(F32)
    for u in range(T):
        after = after + recva[u].astype(F32)
    agf[me_t] = (after * factor_of(after) * consts[1:2, :]).astype(BF16)
    step = tp_exchange(4, lambda peer: agf.at[me_t], agf)
    for i in range(first_ffn, len(loads)):
        loads[i].wait()
    arrive(step)

    rows32 = rows_of(agf, T)
    rows = rows32.astype(BF16)
    outgoing = nn(dispatch, rows)
    for j in range(EP):
        sende[j] = outgoing[cap * j : cap * (j + 1)].astype(BF16)
    step = ep_exchange(0, sende, recve)
    recve[me_e] = sende[me_e]

    act = (silu(nt(rows, v_sg[...])) * nt(rows, v_su[...])).astype(BF16)
    ffn = nn(act, v_sd[...])
    gate = jnp.sum(rows32 * consts[2:3, :], axis=-1, keepdims=True)
    gate = 1.0 / (1.0 + jnp.exp(-gate))
    act = (silu(nn(rows, v_dg[...])) * nn(rows, v_du[...])).astype(BF16)
    ffn = ffn + gate * nn(act, v_dd[...])

    arrive(step)
    routed = rows_of(recve, EP).astype(BF16)
    act = (silu(nn(routed, v_eg[...])) * nn(routed, v_eu[...])).astype(BF16)
    result = nn(act, v_ed[...])
    for j in range(EP):
        sendr[j] = result[cap * j : cap * (j + 1)].astype(BF16)
    step = ep_exchange(1, sendr, recvr)
    recvr[me_e] = sendr[me_e]
    arrive(step)
    returned = rows_of(recvr, EP).astype(BF16)
    ffn = ffn + (tn(weight_hi, returned) + tn(weight_lo, returned))
    for u in range(T):
        sendf[u] = ffn[own * u : own * (u + 1)].astype(BF16)
    step = tp_exchange(5, lambda peer: sendf.at[peer], recvf)
    recvf[me_t] = sendf[me_t]
    arrive(step)
    for u in range(T):
        after = after + recvf[u].astype(F32)
    mixed[...] = after.astype(BF16)
    for c in sends:
        c.wait_send()


def local(
    tokens, lengths, cache_latent, cache_rope_key, route_ids, route_weights, attn_gain,
    w_query_nope, w_query_rope, w_latent_down, w_key_rope, latent_gain, w_key_up, w_value_up,
    w_attn_out, ffn_gain, expert_gate, expert_up, expert_down, shared_gate, shared_up,
    shared_down, dense_gate, dense_up, dense_down, branch_gate,
):
    own, width = tokens.shape
    T = lax.axis_size("tp")
    EP = lax.axis_size("ep")
    H, nope = w_query_nope.shape[1:]
    rope = w_query_rope.shape[2]
    latent = cache_latent.shape[2]
    top = route_ids.shape[1]
    assert expert_gate.shape[0] == 1
    cap = max(2, (2 * own * top + EP - 1) // EP)
    R = H * own
    half = rope // 2

    frequencies = rope_base ** (-jnp.arange(half).astype(F32) / half)
    angles = lengths.astype(F32)[:, None] * frequencies[None, :]
    pad = ((0, 0), (0, lanes - rope))
    cosine = jnp.pad(jnp.tile(jnp.cos(angles), (1, 2)), pad)
    sine = jnp.pad(jnp.tile(jnp.sin(angles), (1, 2)), pad)
    length = jnp.broadcast_to(lengths.astype(F32)[:, None], (own, lanes))
    which = jnp.broadcast_to(jnp.arange(own, dtype=F32)[:, None], (own, lanes))
    tab = jnp.stack([cosine, sine, length, which])
    tab = jnp.tile(tab, (1, T * H, 1))
    consts = jnp.stack(
        [
            attn_gain,
            ffn_gain,
            branch_gate.astype(F32),
            jnp.pad(latent_gain, (0, width - latent)),
        ]
    )

    operands = (
        consts,
        tab,
        tokens,
        route_ids.T,
        route_weights.T,
        w_query_nope.transpose(1, 2, 0).reshape(H * nope, width),
        w_query_rope.transpose(1, 2, 0).reshape(H * rope, width),
        w_latent_down.T,
        w_key_rope.T,
        cache_latent,
        cache_rope_key.transpose(0, 2, 1),
        w_key_up.transpose(1, 2, 0),
        w_value_up.transpose(1, 2, 0),
        w_attn_out,
        shared_gate.T,
        shared_up.T,
        dense_gate,
        dense_up,
        shared_down,
        dense_down,
        expert_gate[0],
        expert_up[0],
        expert_down[0],
    )
    big = operands[5:]
    v_in = pltpu.VMEM((sum(o.shape[0] for o in big[:3]), width), BF16)
    weights = [v_in] + [pltpu.VMEM(o.shape, BF16) for o in big[3:]]
    q_width = latent + 2 * lanes

    def comm(*shape):
        return pltpu.VMEM(shape, BF16)

    buffers = [
        comm(T, own, width),
        comm(T, R, q_width), comm(T, R, q_width),
        comm(T, R, latent), comm(T, R, latent),
        comm(T, own, width), comm(T, own, width),
        comm(T, own, width),
        comm(EP, cap, width), comm(EP, cap, width),
        comm(EP, cap, width), comm(EP, cap, width),
        comm(T, own, width), comm(T, own, width),
        pltpu.VMEM((own, lanes), F32),
    ]
    n_loads = len(big) + own - 1
    sems = [
        pltpu.SemaphoreType.DMA((n_loads,)),
        pltpu.SemaphoreType.DMA((6, T)),
        pltpu.SemaphoreType.DMA((6, T)),
        pltpu.SemaphoreType.DMA((2, EP)),
        pltpu.SemaphoreType.DMA((2, EP)),
    ]
    sizes = (T, EP, own, H, nope, rope, latent, cap, (nope + rope) ** (-0.5))
    vmem = pl.BlockSpec(memory_space=pltpu.VMEM)
    return pl.pallas_call(
        functools.partial(layer, sizes),
        out_shape=(
            jax.ShapeDtypeStruct((own, width), BF16),
            jax.ShapeDtypeStruct((own, latent), BF16),
            jax.ShapeDtypeStruct((own, rope), BF16),
        ),
        in_specs=[vmem] * 5 + [pl.BlockSpec(memory_space=pl.ANY)] * len(big),
        out_specs=(vmem, vmem, vmem),
        scratch_shapes=weights + buffers + sems,
        compiler_params=pltpu.CompilerParams(collective_id=0, has_side_effects=True),
    )(*operands)


def solution(mesh):
    both = ("ep", "tp")
    in_specs = (
        P(both, None),
        P(both),
        P(both, None, None),
        P(both, None, None),
        P("ep", None),
        P("ep", None),
        P(),
        P(None, "tp", None),
        P(None, "tp", None),
        P(None, "tp"),
        P(),
        P(),
        P(None, "tp", None),
        P(None, "tp", None),
        P("tp", None, None),
        P(),
        P(both, None, None),
        P(both, None, None),
        P(both, None, None),
        P(None, "tp"),
        P(None, "tp"),
        P("tp", None),
        P(None, "tp"),
        P(None, "tp"),
        P("tp", None),
        P(),
    )
    out_specs = (P(both, None), P(both, None), P(both, None))
    return jax.shard_map(local, mesh=mesh, in_specs=in_specs, out_specs=out_specs, check_vma=False)
```

time: 223 us -> 56 us (0.25)
  waiting for transfers between devices: 126 us -> 0 us
  Pallas kernels: 0 us -> 46.5 us
  matrix products: 26.3 us -> 0 us
  starting transfers between devices: 23.6 us -> 0 us
  blocking collectives: 15.7 us -> 0 us
  between operations: 15.1 us -> 0.66 us
  other arithmetic: 9.66 us -> 2.83 us
    psum x1 -> x0, waiting for transfers between devices: 53.5 us -> none  [local(): lax.psum((attn_part + placed).astype(jnp.bfloat16), 'tp')]
    unnamed x3 -> x0, waiting for transfers between devices: 51.4 us -> none
    pallas_call x0 -> x1, Pallas kernels: none -> 46.5 us  [local(): pl.pallas_call(functools.partial(layer, sizes), out_shape=(jax.ShapeDtype...]
    dot_general x20 -> x0, matrix products: 26.3 us -> none  [the longest x2 3.66 us: swiglu(): gate_val = jnp.dot(inputs, gate_w, preferred_element_type=jnp.float32)]
    all_to_all x6 -> x0, starting transfers between devices: 23.5 us -> none  [the longest x1 5.11 us: local(): lax.all_to_all(query_rope, 'tp', split_axis=0, concat_axis=1, tiled=True)]
    all_to_all x6 -> x0, waiting for transfers between devices: 21.2 us -> none  [the longest x1 5.38 us: local(): lax.all_to_all(query_latent, 'tp', split_axis=0, concat_axis=1, tiled=True)]
    all_gather x1 -> x0, blocking collectives: 15.7 us -> none  [local(): group_in = lax.all_gather(normed, 'tp', axis=0, tiled=True)]
    reduce_sum x6 -> x0, other arithmetic: 3.23 us -> none  [the longest x3 2.16 us: norm_rows(): jnp.mean(values * values, axis=-1, keepdims=True) + epsilon]
  transfers between devices with their start and end apart: 8 -> 0, of which waited for: 7 -> 0; matrix products, arithmetic and copies ran while one was open for 8% -> 0% of each run, Pallas kernels for 0% -> 0%
where the time goes in v1:
time: 56 us; the launch traced here: 55.4 us
  Pallas kernels  46.5 us (83%)
  local copies, waits for them, and re-layouts  5.41 us (10%)
  other arithmetic  2.83 us (5%)
  between operations  0.66 us (1%)
    pallas_call x1, Pallas kernels, local(): pl.pallas_call(functools.partial(layer, sizes), out_shape=(jax.ShapeDtype...  46.5 us
    unnamed x3, local copies, waits for them, and re-layouts  3.8 us
    another operation x2, other arithmetic, local(): jnp.stack([attn_gain, ffn_gain, branch_gate.astype(F32), jnp.pad(latent_g...  2.05 us

profile of v1, /device:TPU:0, one launch (start us, length us, event | category | flops | bytes accessed | tf_op | source)
XLA Modules:
  0.0 55.4 jit_solution(1662255863462188307)
XLA Ops:
  0.6 0.7 %convert_element_type.17 = f32[4]{0:T(128)S(1)} convert(s32[4]{0:T(128)} %param.27) | non-fusion elementwise | flops 4 | bytes 32 | tf_op jit(solution)/shard_map/convert_element_type | solution.py:342
  1.3 0.1 stack_broadcast_in_dim.4
  1.4 0.1 multiply_cosine_fusion
  1.5 0.1 tile.13
  1.6 0.1 tile.30
  1.7 0.7 %pad.11 = f32[2048]{0:T(1024)S(1)} pad(f32[512]{0:T(512)} %param.37, f32[]{:T(128)} %constant.2.clone.1), padding=0_1536 | pad | bytes 10244 | tf_op jit(solution)/shard_map/jit(_pad)/pad | solution.py:355
  2.4 0.7 %stack.36 = f32[2048]{0:T(1024)S(1)} convert(bf16[2048]{0:T(1024)(128)(2,1)} %param.51) | non-fusion elementwise | flops 2048 | bytes 12288 | tf_op jit(solution)/shard_map/stack | solution.py:350
  3.1 1.4 %pad_maximum_fusion.consts = f32[4,2048]{1,0:T(4,128)} fusion(f32[1,2048]{1,0:T(1,128)S(1)} %bitcast.40, f32[1,2048]{1,0:T(1,128)S(1)} %bitcast.41, f32[1,2048]{1,0:T(1,128)} %bitcast.42, f32[1,2048]{1,0:T(1,128)} %bitcast.43), kind=kLoop, calls=%fused_computation | loop fusion | flops 24576 | bytes 65536 | tf_op jit(solution)/shard_map/stack | solution.py:350
  4.4 0.7 %tile.31 = f32[4,16,4,128]{3,2,1,0:T(4,128)} broadcast(f32[4,4,128]{2,1,0:T(4,128)S(1)} %pad_maximum_fusion.1), dimensions={0,2,3} | broadcast | bytes 139264 | tf_op jit(solution)/shard_map/tile | solution.py:349
  5.1 46.5 %shard_map.265 = (bf16[4,2048]{1,0:T(4,128)(2,1)}, bf16[4,512]{1,0:T(4,128)(2,1)}, bf16[4,32]{1,0:T(4,128)(2,1)}) custom-call(f32[4,2048]{1,0:T(4,128)} %pad_maximum_fusion.consts, f32[4,64,128]{2,1,0:T(8,128)} %bitcast.30, bf16[4,2048]{1,0:T(4,128)(2,1)} %tokens.1, s32[4,32]{1,0:T(4,128)} %bitcast.44, f32[4,32]{1,0:T(4,128)} %bitcast.45, ...), custom_call_target="tpu_custom_call" | custom-call | tf_op jit(solution)/shard_map/pallas_call | solution.py:413
  51.6 1.3 %copy.32 = bf16[4,2048]{1,0:T(4,128)(2,1)} copy(bf16[4,2048]{1,0:T(4,128)(2,1)} %get-tuple-element.10) | data formatting | bytes 32768
  53.0 1.3 %copy.33 = bf16[4,512]{1,0:T(4,128)(2,1)} copy(bf16[4,512]{1,0:T(4,128)(2,1)} %get-tuple-element.11) | data formatting | bytes 8192
  54.2 1.2 %copy.34 = bf16[4,32]{1,0:T(4,128)(2,1)} copy(bf16[4,32]{1,0:T(4,128)(2,1)} %get-tuple-element.12) | data formatting | bytes 512
  (6 shorter events, 0.0 us)

commit v2 on v1

--- a/solution.py
+++ b/solution.py
@@ -2,6 +2,7 @@
 
 import jax
 import jax.numpy as jnp
+import numpy as np
 from jax import lax
 from jax.experimental import pallas as pl
 from jax.experimental.pallas import tpu as pltpu
@@ -29,6 +30,27 @@
 
 def join(pieces):
     return pieces[0] if len(pieces) == 1 else jnp.concatenate(pieces, axis=0)
+
+
+def flipped(index, mask, count):
+    out = index
+    bit = 1
+    while bit < count:
+        if mask & bit:
+            out = out + bit - 2 * bit * (index // bit % 2)
+        bit *= 2
+    return out
+
+
+def flat(ref):
+    return jnp.concatenate([ref[i : i + 1, :] for i in range(ref.shape[0])], axis=1)
+
+
+def spread(values, count):
+    rows = values.shape[0]
+    return join(
+        [jnp.broadcast_to(values[b : b + 1], (count, values.shape[1])) for b in range(rows)]
+    )
 
 
 def rows_of(ref, count):
@@ -62,7 +84,7 @@
 
 def layer(
     sizes,
-    consts, tab, tokens, ids, wts,
+    turns, tokens, ids, wts, attn_gain, ffn_gain, latent_gain, branch_gate, lengths,
     wqn, wqr, wld, wkr, cl, cr, wku, wvu, wo, sg, su, dg, du, sd, dd, eg, eu, ed,
     mixed, newlat, newrope,
     v_in, v_kr, v_cl, v_cr, v_ku, v_vu, v_wo, v_sg, v_su, v_dg, v_du, v_sd, v_dd, v_eg, v_eu, v_ed,
@@ -79,11 +101,11 @@
     barrier = pltpu.get_barrier_semaphore()
     for k in range(1, T):
         pl.semaphore_signal(
-            barrier, inc=1, device_id=(me_e, lax.rem(me_t + k, T)), device_id_type=MESH
+            barrier, inc=1, device_id=(me_e, flipped(me_t, k, T)), device_id_type=MESH
         )
     for k in range(1, EP):
         pl.semaphore_signal(
-            barrier, inc=1, device_id=(lax.rem(me_e + k, EP), me_t), device_id_type=MESH
+            barrier, inc=1, device_id=(flipped(me_e, k, EP), me_t), device_id_type=MESH
         )
 
     n_q, n_r = H * nope, H * rope
@@ -113,8 +135,8 @@
 
     def tp_exchange(phase, source, target):
         out = []
-        for k in range(1, T):
-            peer = lax.rem(me_t + k, T)
+        for k in range(T - 1, 0, -1):
+            peer = flipped(me_t, k, T)
             out.append(
                 pltpu.make_async_remote_copy(
                     src_ref=source(peer),
@@ -132,8 +154,8 @@
 
     def ep_exchange(phase, source, target):
         out = []
-        for k in range(1, EP):
-            peer = lax.rem(me_e + k, EP)
+        for k in range(EP - 1, 0, -1):
+            peer = flipped(me_e, k, EP)
             out.append(
                 pltpu.make_async_remote_copy(
                     src_ref=source.at[peer],
@@ -154,7 +176,7 @@
             c.wait_recv()
 
     x = tokens[...].astype(F32)
-    normed = (x * factor_of(x) * consts[0:1, :]).astype(BF16)
+    normed = (x * factor_of(x) * flat(attn_gain[...])).astype(BF16)
     agx[me_t] = normed
     pl.semaphore_wait(barrier, T - 1 + EP - 1)
     step = tp_exchange(0, lambda peer: agx.at[me_t], agx)
@@ -187,10 +209,40 @@
 
     for i in range(first_cl):
         loads[i].wait()
-    cosine, sine = tab[0], tab[1]
+    left = jnp.zeros((own, lanes), jnp.int32)
+    row = lax.broadcasted_iota(jnp.int32, (own, lanes), 0)
+    for b in range(own):
+        left = jnp.where(row == b, lengths[b], left)
+    length = left
+    bits = turns.shape[0] // 2
+    cosine = jnp.ones((own, lanes), F32)
+    sine = jnp.zeros((own, lanes), F32)
+    for i in range(bits - 1, -1, -1):
+        has = left >= 2**i
+        left = jnp.where(has, left - 2**i, left)
+        c, s = turns[i : i + 1, :], turns[bits + i : bits + i + 1, :]
+        cosine, sine = (
+            jnp.where(has, cosine * c - sine * s, cosine),
+            jnp.where(has, cosine * s + sine * c, sine),
+        )
+    live = lax.broadcasted_iota(jnp.int32, (own, lanes), 1) < rope
+    cosine = jnp.where(live, cosine, 0.0)
+    sine = jnp.where(live, sine, 0.0)
+    big = T * H
+    at = lax.broadcasted_iota(jnp.int32, (own * big, own * big), 0)
+    to = lax.broadcasted_iota(jnp.int32, (own * big, own * big), 1)
+
+    def from_row(r):
+        seq = jnp.zeros_like(r)
+        for i in range(1, own):
+            seq = seq + jnp.where(r >= i * big, 1, 0)
+        return (r - seq * big) * own + seq
+
+    to_seq = jnp.where(to == from_row(at), 1.0, 0.0).astype(BF16)
+    to_dev = jnp.where(at == from_row(to), 1.0, 0.0).astype(BF16)
     kr_pad[...] = jnp.zeros_like(kr_pad)
     kr_pad[:, 0:rope] = nt(normed, v_kr[...])
-    new_rope = turn(kr_pad[...], cosine[0:own], sine[0:own], rope // 2).astype(BF16)
+    new_rope = turn(kr_pad[...], cosine, sine, rope // 2).astype(BF16)
     newrope[...] = new_rope[:, 0:rope]
 
     arrive(step)
@@ -200,12 +252,13 @@
         nn(lane_block(proj, h * nope, nope)[:, 0:nope].astype(BF16), v_ku[h]) for h in range(H)
     ]
     q_rope = [lane_block(proj, n_q + h * rope, rope) for h in range(H)]
-    lat_part = lane_block(proj, n_q + n_r, lat_w)
+    lat_part = pltpu.roll(lane_block(proj, n_q + n_r, lat_w), lanes - lat_w, 1)
     for u in range(T):
         cut = slice(own * u, own * (u + 1))
         sendq[u, :, 0:latent] = join([q[cut] for q in q_lat]).astype(BF16)
-        sendq[u, :, latent : latent + lanes] = join([q[cut] for q in q_rope]).astype(BF16)
-        sendq[u, :, latent + lanes : latent + 2 * lanes] = join([lat_part[cut]] * H).astype(BF16)
+        sendq[u, :, latent : latent + lanes] = join(
+            [q[cut] + lat_part[cut] for q in q_rope]
+        ).astype(BF16)
     step = tp_exchange(1, lambda peer: sendq.at[peer], recvq)
     recvq[me_t] = sendq[me_t]
     for i in range(first_cl, first_ffn):
@@ -213,46 +266,52 @@
     arrive(step)
 
     queries = rows_of(recvq, T)
-    q_all = queries[:, 0:latent].astype(BF16)
-    q_rot = turn(queries[:, latent : latent + lanes], cosine, sine, rope // 2).astype(BF16)
     per = lanes // lat_w
+    lane = lax.broadcasted_iota(jnp.int32, (own, lanes), 1)
     blocks = []
     for j in range(T // per):
         total = None
         for i in range(per):
-            piece = queries[R * (j * per + i) : R * (j * per + i) + own, latent + lanes :]
-            if i:
-                piece = pltpu.roll(piece, i * lat_w, 1)
+            top = R * (j * per + i)
+            piece = jnp.where(lane >= lanes - lat_w, queries[top : top + own, latent:], 0.0)
+            if i < per - 1:
+                piece = pltpu.roll(piece, (i + 1) * lat_w, 1)
             total = piece if total is None else total + piece
         blocks.append(total)
     raw = blocks[0] if len(blocks) == 1 else jnp.concatenate(blocks, axis=1)
-    new_latent = (raw * factor_of(raw) * consts[3:4, 0:latent]).astype(BF16)
+    new_latent = (raw * factor_of(raw) * flat(latent_gain[...])).astype(BF16)
     newlat[...] = new_latent
-    lat_rows = join([new_latent.astype(F32)] * (T * H))
-    rope_rows = join([new_rope.astype(F32)] * (T * H))
-    own_score = (
-        jnp.sum(q_all.astype(F32) * lat_rows, axis=-1, keepdims=True)
-        + jnp.sum(q_rot.astype(F32) * rope_rows, axis=-1, keepdims=True)
-    ) * scale
-    length = tab[2][:, 0:1]
-    which = tab[3][:, 0:1]
-    scores = None
+    new_lat32, new_rope32 = new_latent.astype(F32), new_rope.astype(F32)
+    queries = nn(to_seq, queries.astype(BF16))
+    q_rot = turn(
+        jnp.where(
+            lax.broadcasted_iota(jnp.int32, (own * big, lanes), 1) < rope, queries[:, latent:], 0.0
+        ),
+        spread(cosine, big),
+        spread(sine, big),
+        rope // 2,
+    ).astype(BF16)
+    q_lat32 = queries[:, 0:latent]
+    outs = []
     for b in range(own):
-        part = nt(q_all, v_cl[b]) + nn(q_rot[:, 0:rope], v_cr[b])
-        scores = part if scores is None else jnp.where(which == float(b), part, scores)
-    position = lax.broadcasted_iota(jnp.int32, scores.shape, 1).astype(F32)
-    scores = jnp.where(position < length, scores * scale, -jnp.inf)
-    peak = jnp.maximum(jnp.max(scores, axis=-1, keepdims=True), own_score)
-    past = jnp.exp(scores - peak)
-    own_exp = jnp.exp(own_score - peak)
-    total = jnp.sum(past, axis=-1, keepdims=True) + own_exp
-    past = (past / total).astype(BF16)
-    own_weight = (own_exp / total).astype(BF16).astype(F32)
-    mixed_lat = None
-    for b in range(own):
-        part = nn(past, v_cl[b])
-        mixed_lat = part if mixed_lat is None else jnp.where(which == float(b), part, mixed_lat)
-    mixed_lat = mixed_lat + own_weight * lat_rows
+        cut = slice(big * b, big * (b + 1))
+        q_b, r_b = q_lat32[cut], q_rot.astype(F32)[cut]
+        lat_b, rope_b = new_lat32[b : b + 1], new_rope32[b : b + 1]
+        own_score = (
+            jnp.sum(q_b * lat_b, axis=-1, keepdims=True)
+            + jnp.sum(r_b * rope_b, axis=-1, keepdims=True)
+        ) * scale
+        scores = nt(q_b.astype(BF16), v_cl[b]) + nn(r_b[:, 0:rope].astype(BF16), v_cr[b])
+        position = lax.broadcasted_iota(jnp.int32, scores.shape, 1)
+        scores = jnp.where(position < length[b : b + 1, 0:1], scores * scale, -jnp.inf)
+        peak = jnp.maximum(jnp.max(scores, axis=-1, keepdims=True), own_score)
+        past = jnp.exp(scores - peak)
+        own_exp = jnp.exp(own_score - peak)
+        total = jnp.sum(past, axis=-1, keepdims=True) + own_exp
+        past = (past / total).astype(BF16)
+        own_weight = (own_exp / total).astype(BF16).astype(F32)
+        outs.append(nn(past, v_cl[b]) + own_weight * lat_b)
+    mixed_lat = nn(to_dev, join(outs).astype(BF16))
     for u in range(T):
         sendo[u] = mixed_lat[R * u : R * (u + 1)].astype(BF16)
     step = tp_exchange(2, lambda peer: sendo.at[peer], recvo)
@@ -276,7 +335,7 @@
     after = tokens[...].astype(F32)
     for u in range(T):
         after = after + recva[u].astype(F32)
-    agf[me_t] = (after * factor_of(after) * consts[1:2, :]).astype(BF16)
+    agf[me_t] = (after * factor_of(after) * flat(ffn_gain[...])).astype(BF16)
     step = tp_exchange(4, lambda peer: agf.at[me_t], agf)
     for i in range(first_ffn, len(loads)):
         loads[i].wait()
@@ -292,7 +351,7 @@
 
     act = (silu(nt(rows, v_sg[...])) * nt(rows, v_su[...])).astype(BF16)
     ffn = nn(act, v_sd[...])
-    gate = jnp.sum(rows32 * consts[2:3, :], axis=-1, keepdims=True)
+    gate = jnp.sum(rows32 * flat(branch_gate[...].astype(F32)), axis=-1, keepdims=True)
     gate = 1.0 / (1.0 + jnp.exp(-gate))
     act = (silu(nn(rows, v_dg[...])) * nn(rows, v_du[...])).astype(BF16)
     ffn = ffn + gate * nn(act, v_dd[...])
@@ -318,6 +377,12 @@
     mixed[...] = after.astype(BF16)
     for c in sends:
         c.wait_send()
+
+
+def hand_over(*refs):
+    half = len(refs) // 2
+    for source, target in zip(refs[:half], refs[half:]):
+        target[...] = source[...]
 
 
 def local(
@@ -338,30 +403,22 @@
     R = H * own
     half = rope // 2
 
-    frequencies = rope_base ** (-jnp.arange(half).astype(F32) / half)
-    angles = lengths.astype(F32)[:, None] * frequencies[None, :]
-    pad = ((0, 0), (0, lanes - rope))
-    cosine = jnp.pad(jnp.tile(jnp.cos(angles), (1, 2)), pad)
-    sine = jnp.pad(jnp.tile(jnp.sin(angles), (1, 2)), pad)
-    length = jnp.broadcast_to(lengths.astype(F32)[:, None], (own, lanes))
-    which = jnp.broadcast_to(jnp.arange(own, dtype=F32)[:, None], (own, lanes))
-    tab = jnp.stack([cosine, sine, length, which])
-    tab = jnp.tile(tab, (1, T * H, 1))
-    consts = jnp.stack(
-        [
-            attn_gain,
-            ffn_gain,
-            branch_gate.astype(F32),
-            jnp.pad(latent_gain, (0, width - latent)),
-        ]
-    )
+    bits = cache_latent.shape[1].bit_length()
+    frequencies = (rope_base ** (-np.arange(half) / half)).astype(np.float32).astype(np.float64)
+    angles = frequencies[None, :] * 2.0 ** np.arange(bits)[:, None]
+    angles = np.pad(np.tile(angles, (1, 2)), ((0, 0), (0, lanes - rope)))
+    turns = jnp.asarray(np.concatenate([np.cos(angles), np.sin(angles)]), F32)
 
     operands = (
-        consts,
-        tab,
+        turns,
         tokens,
         route_ids.T,
         route_weights.T,
+        attn_gain.reshape(-1, lanes),
+        ffn_gain.reshape(-1, lanes),
+        latent_gain.reshape(-1, lanes),
+        branch_gate.reshape(-1, lanes),
+        lengths,
         w_query_nope.transpose(1, 2, 0).reshape(H * nope, width),
         w_query_rope.transpose(1, 2, 0).reshape(H * rope, width),
         w_latent_down.T,
@@ -381,10 +438,10 @@
         expert_up[0],
         expert_down[0],
     )
-    big = operands[5:]
+    big = operands[9:]
     v_in = pltpu.VMEM((sum(o.shape[0] for o in big[:3]), width), BF16)
     weights = [v_in] + [pltpu.VMEM(o.shape, BF16) for o in big[3:]]
-    q_width = latent + 2 * lanes
+    q_width = latent + lanes
 
     def comm(*shape):
         return pltpu.VMEM(shape, BF16)
@@ -410,18 +467,26 @@
     ]
     sizes = (T, EP, own, H, nope, rope, latent, cap, (nope + rope) ** (-0.5))
     vmem = pl.BlockSpec(memory_space=pltpu.VMEM)
-    return pl.pallas_call(
+    results = pl.pallas_call(
         functools.partial(layer, sizes),
         out_shape=(
             jax.ShapeDtypeStruct((own, width), BF16),
             jax.ShapeDtypeStruct((own, latent), BF16),
             jax.ShapeDtypeStruct((own, rope), BF16),
         ),
-        in_specs=[vmem] * 5 + [pl.BlockSpec(memory_space=pl.ANY)] * len(big),
+        in_specs=[vmem] * 8
+        + [pl.BlockSpec(memory_space=pltpu.SMEM)]
+        + [pl.BlockSpec(memory_space=pl.ANY)] * len(big),
         out_specs=(vmem, vmem, vmem),
         scratch_shapes=weights + buffers + sems,
         compiler_params=pltpu.CompilerParams(collective_id=0, has_side_effects=True),
     )(*operands)
+    return pl.pallas_call(
+        hand_over,
+        out_shape=tuple(jax.ShapeDtypeStruct(r.shape, r.dtype) for r in results),
+        in_specs=[vmem] * 3,
+        out_specs=(vmem, vmem, vmem),
+    )(*results)
 
 
 def solution(mesh):

time: 56 us -> 49.9 us (0.89)
  local copies, waits for them, and re-layouts: 5.41 us -> 0 us
  other arithmetic: 2.83 us -> 0 us
  Pallas kernels: 46.5 us -> 49 us
    unnamed x3 -> x0, local copies, waits for them, and re-layouts: 3.8 us -> none
    another operation x3 -> x0, other arithmetic: 2.06 us -> none  [the longest x2 2.05 us: local(): jnp.stack([attn_gain, ffn_gain, branch_gate.astype(F32), jnp.pad(latent_g...]
    pallas_call x0 -> x1, Pallas kernels: none -> 1.34 us  [local(): pl.pallas_call(hand_over, out_shape=tuple((jax.ShapeDtypeStruct(r.shape,...]
    pallas_call x1, Pallas kernels: 46.5 us -> 47.7 us  [local(): pl.pallas_call(functools.partial(layer, sizes), out_shape=(jax.ShapeDtype...]
    another operation x8 -> x0, local copies, waits for them, and re-layouts: 0.92 us -> none  [the longest x1 0.66 us: local(): tab = jnp.tile(tab, (1, T * H, 1))]
    pad x1 -> x0, local copies, waits for them, and re-layouts: 0.69 us -> none  [local(): jnp.pad(latent_gain, (0, width - latent))]
    convert_element_type x1 -> x0, other arithmetic: 0.66 us -> none  [local(): angles = lengths.astype(F32)[:, None] * frequencies[None, :]]
where the time goes in v2:
time: 49.9 us; the launch traced here: 49.7 us
  Pallas kernels  49 us (98%)
  between operations  0.65 us (1%)
    pallas_call x1, Pallas kernels, local(): pl.pallas_call(functools.partial(layer, sizes), out_shape=(jax.ShapeDtype...  47.7 us
    pallas_call x1, Pallas kernels, local(): pl.pallas_call(hand_over, out_shape=tuple((jax.ShapeDtypeStruct(r.shape,...  1.34 us

profile of v2, /device:TPU:0, one launch (start us, length us, event | category | flops | bytes accessed | tf_op | source)
XLA Modules:
  0.0 49.7 jit_solution(4964366726004234605)
XLA Ops:
  0.6 47.7 %shard_map.274 = (bf16[4,2048]{1,0:T(4,128)(2,1)}, bf16[4,512]{1,0:T(4,128)(2,1)}, bf16[4,32]{1,0:T(4,128)(2,1)}) custom-call(f32[22,128]{1,0:T(8,128)} %constant.2.clone.turns, bf16[4,2048]{1,0:T(4,128)(2,1)} %tokens.1, s32[4,32]{1,0:T(4,128)} %bitcast.37, f32[4,32]{1,0:T(4,128)} %bitcast.38, f32[16,128]{1,0:T(8,128)} %bitcast.34, f32[16,128]{1,0:T(8,128)} %bitcast.35, ...), custom_call_target="tpu_custom_call" | custom-call | tf_op jit(solution)/shard_map/pallas_call | solution.py:470
  48.3 1.3 %shard_map.275 = (bf16[4,2048]{1,0:T(4,128)(2,1)}, bf16[4,512]{1,0:T(4,128)(2,1)}, bf16[4,32]{1,0:T(4,128)(2,1)}) custom-call(bf16[4,2048]{1,0:T(4,128)(2,1)} %get-tuple-element.6.refs_0_, bf16[4,512]{1,0:T(4,128)(2,1)} %get-tuple-element.7.refs_1_, bf16[4,32]{1,0:T(4,128)(2,1)} %get-tuple-element.8.refs_2_), custom_call_target="tpu_custom_call" | custom-call | tf_op jit(solution)/shard_map/pallas_call | solution.py:484

commit v3 on v2

--- a/solution.py
+++ b/solution.py
@@ -89,6 +89,7 @@
     mixed, newlat, newrope,
     v_in, v_kr, v_cl, v_cr, v_ku, v_vu, v_wo, v_sg, v_su, v_dg, v_du, v_sd, v_dd, v_eg, v_eu, v_ed,
     agx, sendq, recvq, sendo, recvo, senda, recva, agf, sende, recve, sendr, recvr, sendf, recvf,
+    half_a, whole_a,
     kr_pad, w_sem, tp_send, tp_recv, ep_send, ep_recv,
 ):
     T, EP, own, H, nope, rope, latent, cap, scale = sizes
@@ -152,6 +153,59 @@
         sends.extend(out)
         return out
 
+    def tp_copy(phase, k, source, target, peer):
+        c = pltpu.make_async_remote_copy(
+            src_ref=source,
+            dst_ref=target,
+            send_sem=tp_send.at[phase, k],
+            recv_sem=tp_recv.at[phase, k],
+            device_id=(me_e, peer),
+            device_id_type=MESH,
+        )
+        c.start()
+        sends.append(c)
+        return c
+
+    partner = flipped(me_t, 1, T)
+    across = list(range(T - 2, 0, -2))
+
+    def tp_gather(phase, target):
+        mine = target.at[me_t]
+        direct = [(m, tp_copy(phase, m, mine, mine, flipped(me_t, m, T))) for m in across]
+        out = [tp_copy(phase, 1, mine, mine, partner)]
+
+        def finish():
+            for m, c in reversed(direct):
+                c.wait_recv()
+                block = target.at[flipped(me_t, m, T)]
+                out.append(tp_copy(phase, m + 1, block, block, partner))
+            for c in out:
+                c.wait_recv()
+
+        return finish
+
+    def tp_scatter(phase, source, half, whole, target):
+        first = []
+        for m in across + [0]:
+            to = flipped(partner, m, T)
+            first.append((m, tp_copy(phase, m + 1, source.at[to], half.at[to], partner)))
+        out = []
+        for m, c in first:
+            c.wait_recv()
+            to = flipped(me_t, m, T)
+            both = (source[to].astype(F32) + half[to].astype(F32)).astype(BF16)
+            if m == 0:
+                target[me_t] = both
+            else:
+                whole[to] = both
+                out.append(tp_copy(phase, m, whole.at[to], target.at[me_t], to))
+        for c in out:
+            c.wait_recv()
+        total = target[me_t].astype(F32)
+        for m in across:
+            total = total + target[flipped(me_t, m, T)].astype(F32)
+        return total
+
     def ep_exchange(phase, source, target):
         out = []
         for k in range(EP - 1, 0, -1):
@@ -179,7 +233,7 @@
     normed = (x * factor_of(x) * flat(attn_gain[...])).astype(BF16)
     agx[me_t] = normed
     pl.semaphore_wait(barrier, T - 1 + EP - 1)
-    step = tp_exchange(0, lambda peer: agx.at[me_t], agx)
+    finish = tp_gather(0, agx)
 
     slots = EP * cap
     slot = lax.broadcasted_iota(jnp.int32, (slots, group), 0)
@@ -245,7 +299,7 @@
     new_rope = turn(kr_pad[...], cosine, sine, rope // 2).astype(BF16)
     newrope[...] = new_rope[:, 0:rope]
 
-    arrive(step)
+    finish()
     rows = rows_of(agx, T).astype(BF16)
     proj = nt(rows, v_in[...])
     q_lat = [
@@ -329,17 +383,12 @@
         part = term if part is None else part + term
     for u in range(T):
         senda[u] = part[own * u : own * (u + 1)].astype(BF16)
-    step = tp_exchange(3, lambda peer: senda.at[peer], recva)
-    recva[me_t] = senda[me_t]
-    arrive(step)
-    after = tokens[...].astype(F32)
-    for u in range(T):
-        after = after + recva[u].astype(F32)
+    after = tokens[...].astype(F32) + tp_scatter(3, senda, half_a, whole_a, recva)
     agf[me_t] = (after * factor_of(after) * flat(ffn_gain[...])).astype(BF16)
-    step = tp_exchange(4, lambda peer: agf.at[me_t], agf)
+    finish = tp_gather(4, agf)
     for i in range(first_ffn, len(loads)):
         loads[i].wait()
-    arrive(step)
+    finish()
 
     rows32 = rows_of(agf, T)
     rows = rows32.astype(BF16)
@@ -359,22 +408,30 @@
     arrive(step)
     routed = rows_of(recve, EP).astype(BF16)
     act = (silu(nn(routed, v_eg[...])) * nn(routed, v_eu[...])).astype(BF16)
-    result = nn(act, v_ed[...])
-    for j in range(EP):
-        sendr[j] = result[cap * j : cap * (j + 1)].astype(BF16)
-    step = ep_exchange(1, sendr, recvr)
-    recvr[me_e] = sendr[me_e]
-    arrive(step)
-    returned = rows_of(recvr, EP).astype(BF16)
-    ffn = ffn + (tn(weight_hi, returned) + tn(weight_lo, returned))
-    for u in range(T):
-        sendf[u] = ffn[own * u : own * (u + 1)].astype(BF16)
-    step = tp_exchange(5, lambda peer: sendf.at[peer], recvf)
-    recvf[me_t] = sendf[me_t]
-    arrive(step)
-    for u in range(T):
-        after = after + recvf[u].astype(F32)
-    mixed[...] = after.astype(BF16)
+    wide = v_ed.shape[1] // 2
+    cuts = [slice(0, wide), slice(wide, 2 * wide)]
+    steps = []
+    for n, cut in enumerate(cuts):
+        result = nn(act, v_ed[:, cut])
+        for j in range(EP):
+            sendr[n, j] = result[cap * j : cap * (j + 1)].astype(BF16)
+        steps.append(ep_exchange(1 + n, sendr.at[n], recvr.at[n]))
+        recvr[n, me_e] = sendr[n, me_e]
+    last = []
+    for n, cut in enumerate(cuts):
+        arrive(steps[n])
+        returned = rows_of(recvr.at[n], EP).astype(BF16)
+        part = ffn[:, cut] + (tn(weight_hi, returned) + tn(weight_lo, returned))
+        for u in range(T):
+            sendf[n, u] = part[own * u : own * (u + 1)].astype(BF16)
+        last.append(tp_exchange(5 + n, lambda peer: sendf.at[n, peer], recvf.at[n]))
+        recvf[n, me_t] = sendf[n, me_t]
+    for n, cut in enumerate(cuts):
+        arrive(last[n])
+        part = after[:, cut]
+        for u in range(T):
+            part = part + recvf[n, u].astype(F32)
+        mixed[:, cut] = part.astype(BF16)
     for c in sends:
         c.wait_send()
 
@@ -453,17 +510,18 @@
         comm(T, own, width), comm(T, own, width),
         comm(T, own, width),
         comm(EP, cap, width), comm(EP, cap, width),
-        comm(EP, cap, width), comm(EP, cap, width),
+        comm(2, EP, cap, width // 2), comm(2, EP, cap, width // 2),
+        comm(2, T, own, width // 2), comm(2, T, own, width // 2),
         comm(T, own, width), comm(T, own, width),
         pltpu.VMEM((own, lanes), F32),
     ]
     n_loads = len(big) + own - 1
     sems = [
         pltpu.SemaphoreType.DMA((n_loads,)),
-        pltpu.SemaphoreType.DMA((6, T)),
-        pltpu.SemaphoreType.DMA((6, T)),
-        pltpu.SemaphoreType.DMA((2, EP)),
-        pltpu.SemaphoreType.DMA((2, EP)),
+        pltpu.SemaphoreType.DMA((7, T)),
+        pltpu.SemaphoreType.DMA((7, T)),
+        pltpu.SemaphoreType.DMA((3, EP)),
+        pltpu.SemaphoreType.DMA((3, EP)),
     ]
     sizes = (T, EP, own, H, nope, rope, latent, cap, (nope + rope) ** (-0.5))
     vmem = pl.BlockSpec(memory_space=pltpu.VMEM)

time: 49.9 us -> 49.2 us (0.986)
  Pallas kernels: 49 us -> 48.3 us
    pallas_call x1, Pallas kernels: 47.7 us -> 47 us  [local(): pl.pallas_call(functools.partial(layer, sizes), out_shape=(jax.ShapeDtype...]
where the time goes in v3:
time: 49.2 us; the launch traced here: 48.9 us
  Pallas kernels  48.3 us (98%)
  between operations  0.65 us (1%)
    pallas_call x1, Pallas kernels, local(): pl.pallas_call(functools.partial(layer, sizes), out_shape=(jax.ShapeDtype...  47 us
    pallas_call x1, Pallas kernels, local(): pl.pallas_call(hand_over, out_shape=tuple((jax.ShapeDtypeStruct(r.shape,...  1.34 us

profile of v3, /device:TPU:0, one launch (start us, length us, event | category | flops | bytes accessed | tf_op | source)
XLA Modules:
  0.0 48.9 jit_solution(13548703662087857609)
XLA Ops:
  0.6 47.0 %shard_map.274 = (bf16[4,2048]{1,0:T(4,128)(2,1)}, bf16[4,512]{1,0:T(4,128)(2,1)}, bf16[4,32]{1,0:T(4,128)(2,1)}) custom-call(f32[22,128]{1,0:T(8,128)} %constant.2.clone.turns, bf16[4,2048]{1,0:T(4,128)(2,1)} %tokens.1, s32[4,32]{1,0:T(4,128)} %bitcast.37, f32[4,32]{1,0:T(4,128)} %bitcast.38, f32[16,128]{1,0:T(8,128)} %bitcast.34, f32[16,128]{1,0:T(8,128)} %bitcast.35, ...), custom_call_target="tpu_custom_call" | custom-call | tf_op jit(solution)/shard_map/pallas_call | solution.py:528
  47.6 1.3 %shard_map.275 = (bf16[4,2048]{1,0:T(4,128)(2,1)}, bf16[4,512]{1,0:T(4,128)(2,1)}, bf16[4,32]{1,0:T(4,128)(2,1)}) custom-call(bf16[4,2048]{1,0:T(4,128)(2,1)} %get-tuple-element.6.refs_0_, bf16[4,512]{1,0:T(4,128)(2,1)} %get-tuple-element.7.refs_1_, bf16[4,32]{1,0:T(4,128)(2,1)} %get-tuple-element.8.refs_2_), custom_call_target="tpu_custom_call" | custom-call | tf_op jit(solution)/shard_map/pallas_call | solution.py:542
